TPU v7x, 512 devices: a whole 4x4x16 slice. The times are simulated.
512 devices in a mesh: sp: 16 (over z), dp: 32 (over y, x, core).
Axes of the slice: x: 4, y: 4, z: 16, core: 2. Of those that a mesh axis runs over, the one named last changes fastest.
Arguments:
- queries: bfloat16 [32, 2048, 1024], P('dp', 'sp'), may hold values from -6 to 6
- key_rows: bfloat16 [32, 2048, 1024], P('dp', 'sp'), may hold values from -6 to 6
- value_rows: bfloat16 [32, 2048, 1024], P('dp', 'sp'), may hold values from -6 to 6
- break_offset: bfloat16 [32, 2048, 16], P('dp', 'sp'), may hold values from 1.5 to 15
- hidden_in: bfloat16 [32, 2048, 2048], P('dp', 'sp'), may hold values from -6 to 6
- gate_weight: bfloat16 [2048, 1024], P('dp', 'sp'), may hold values from -0.125 to 0.125
- out_weight: bfloat16 [1024, 2048], P('sp', 'dp'), may hold values from -0.1875 to 0.1875
Outputs:
- mixed: bfloat16 [32, 2048, 2048], P('dp', 'sp')
All inputs are finite; a program needn't handle non-finite values.
Results may differ from a plain program's by a relative error of at most 0.0063.
Values may be sent and summed in bfloat16 or wider, within the bound.
No kernel may reach another device: no remote copies, remote signals or barrier semaphores. Data moves between devices by JAX's collectives and lax.ppermute only.
A program may use at most 64 MiB of HBM per device.

v0:
```python
import jax
import jax.numpy as jnp
from jax import lax
from jax.sharding import PartitionSpec as P

eps_norm = 1e-05


def turned_gather(arrays, axis, dims):
    turned = [jnp.moveaxis(a, dim, 0) for a, dim in zip(arrays, dims)]
    widths = [t[0].size for t in turned]
    both = jnp.concatenate([t.reshape(-1, w) for t, w in zip(turned, widths)], axis=1)
    out = lax.all_gather(both, axis, axis=0, tiled=True)
    blocks = jnp.split(out, [sum(widths[:k]) for k in range(1, len(widths))], axis=1)
    return tuple(
        (
            jnp.moveaxis(b.reshape(-1, *t.shape[1:]), 0, dim)
            for b, t, dim in zip(blocks, turned, dims)
        )
    )


def stick_blocks(head_queries, head_keys, head_values, head_offsets):
    groups, length, head_size = head_queries.shape
    block_rows = min(512, length)
    block_count = length // block_rows
    score_scale = head_size ** (-0.5)
    query_blocks = head_queries.reshape(groups, block_count, block_rows, head_size)

    def one_block(block_index):
        query_block = lax.dynamic_index_in_dim(query_blocks, block_index, 1, keepdims=False)
        query_pos = block_index * block_rows + jnp.arange(block_rows, dtype=jnp.int32)

        def key_step(step_turn, carry):
            running, carried = carry
            key_first = (block_index - step_turn) * block_rows
            key_block = lax.dynamic_slice_in_dim(head_keys, key_first, block_rows, 1)
            value_block = lax.dynamic_slice_in_dim(head_values, key_first, block_rows, 1)
            offset_block = lax.dynamic_slice_in_dim(head_offsets, key_first, block_rows, 1)
            scores = jnp.einsum(
                "gqd,gkd->gqk", query_block, key_block, preferred_element_type=jnp.float32
            )
            scores = scores * score_scale - offset_block[:, None, :]
            key_pos = key_first + jnp.arange(block_rows, dtype=jnp.int32)
            earlier = key_pos[None, :] < query_pos[:, None]
            keep_log = jnp.where(earlier, jax.nn.log_sigmoid(-scores), 0.0)
            later_sum = lax.cumsum(keep_log, axis=2, reverse=True) - keep_log + carried
            weights = jnp.where(
                earlier, jnp.exp(jax.nn.log_sigmoid(scores) + later_sum), 0.0
            ).astype(jnp.bfloat16)
            running = running + jnp.einsum(
                "gqk,gkd->gqd", weights, value_block, preferred_element_type=jnp.float32
            )
            carried = carried + jnp.sum(keep_log, axis=2, keepdims=True)
            return (running, carried)

        start_carry = (
            jnp.zeros((groups, block_rows, head_size), jnp.float32),
            jnp.zeros((groups, block_rows, 1), jnp.float32),
        )
        running, carried = lax.fori_loop(0, block_index + 1, key_step, start_carry)
        return running

    outputs = lax.map(one_block, jnp.arange(block_count, dtype=jnp.int32))
    return outputs.transpose(1, 0, 2, 3).reshape(groups, length, head_size)


def attend(pieces):
    head_queries, head_keys, head_values, head_offsets = pieces
    item_count, length, feature_count = head_queries.shape
    heads_dev = head_offsets.shape[2]
    head_size = feature_count // heads_dev

    def split_heads(array):
        return (
            array.reshape(item_count, length, heads_dev, head_size)
            .transpose(0, 2, 1, 3)
            .reshape(item_count * heads_dev, length, head_size)
        )

    offsets = (
        head_offsets.transpose(0, 2, 1).reshape(item_count * heads_dev, length).astype(jnp.float32)
    )
    heads_out = stick_blocks(
        split_heads(head_queries), split_heads(head_keys), split_heads(head_values), offsets
    )
    mean_sq = jnp.mean(heads_out * heads_out, axis=2, keepdims=True)
    normed = (heads_out * lax.rsqrt(mean_sq + eps_norm)).astype(jnp.bfloat16)
    return (
        normed.reshape(item_count, heads_dev, length, head_size)
        .transpose(0, 2, 1, 3)
        .reshape(item_count, length, feature_count)
    )


def shards(queries, key_rows, value_rows, break_offset, hidden_in, gate_weight, out_weight):
    tokens = hidden_in[0]
    gate_rows, out_cols = turned_gather((gate_weight, out_weight), "sp", (1, 0))
    gate_pre = jnp.dot(
        tokens,
        lax.all_gather(gate_rows, "dp", axis=0, tiled=True),
        preferred_element_type=jnp.float32,
    )
    gate_act = jax.nn.silu(gate_pre)
    normed = attend(
        (
            lax.all_to_all(queries, "sp", split_axis=2, concat_axis=1, tiled=True),
            lax.all_to_all(key_rows, "sp", split_axis=2, concat_axis=1, tiled=True),
            lax.all_to_all(value_rows, "sp", split_axis=2, concat_axis=1, tiled=True),
            lax.all_to_all(break_offset, "sp", split_axis=2, concat_axis=1, tiled=True),
        )
    )
    returned = lax.all_to_all(normed, "sp", split_axis=1, concat_axis=2, tiled=True)
    gated_rows = (returned[0].astype(jnp.float32) * gate_act).astype(jnp.bfloat16)
    mixed_rows = jnp.dot(
        gated_rows,
        lax.all_gather(out_cols, "dp", axis=1, tiled=True),
        preferred_element_type=jnp.float32,
    )
    return mixed_rows.astype(jnp.bfloat16)[None]


def solution(mesh):
    return jax.shard_map(
        shards,
        mesh=mesh,
        in_specs=(
            P("dp", "sp", None),
            P("dp", "sp", None),
            P("dp", "sp", None),
            P("dp", "sp", None),
            P("dp", "sp", None),
            P("dp", "sp"),
            P("sp", "dp"),
        ),
        out_specs=P("dp", "sp", None),
        check_vma=False,
    )
```

profile of v0, /device:TPU:54, one launch (start us, length us, event | category | flops | bytes accessed | tf_op | source)
XLA Modules:
  0.0 296.1 jit_solution(12190595315451277451)
XLA Ops:
  8.2 34.7 %all_gather.9 = bf16[1024,128]{1,0:T(8,128)(2,1)S(1)} all-gather(bf16[64,128]{1,0:T(8,128)(2,1)S(1)} %pad_maximum_fusion), channel_id=1, replica_groups=mesh['sp'=16,'dp'=32] {'sp'}, dimensions={0}, use_global_device_ids=true | all-gather | bytes 278528 | tf_op jit(solution)/shard_map/all_gather | solution.py:13
  45.1 8.9 %all-to-all-start.2 = ((bf16[1,128,16]{1,0,2:T(2,128)(2,1)}), bf16[1,128,16]{1,0,2:T(2,128)(2,1)S(1)}, u32[]{:S(2)}, u32[]{:S(2)}) async-start(bf16[1,128,16]{1,0,2:T(2,128)(2,1)} %copy.78), calls=%async_computation.2 | async-start | bytes 16384 | tf_op jit(solution)/shard_map/all_to_all | solution.py:110
  55.9 2.3 reduce.6
  58.9 6.1 %all-to-all-done.2 = bf16[1,128,16]{1,0,2:T(2,128)(2,1)S(1)} async-done(((bf16[1,128,16]{1,0,2:T(2,128)(2,1)}), bf16[1,128,16]{1,0,2:T(2,128)(2,1)S(1)}, u32[]{:S(2)}, u32[]{:S(2)}) %all-to-all-start.2) | async-done | bytes 4128 | tf_op jit(solution)/shard_map/all_to_all | solution.py:110
  65.1 5.9 %all-to-all-start.3 = ((bf16[16,2,4096]{2,1,0:T(2,128)(2,1)}), bf16[16,2,4096]{2,1,0:T(2,128)(2,1)S(1)}, u32[]{:S(2)}, u32[]{:S(2)}) async-start(bf16[16,2,4096]{2,1,0:T(2,128)(2,1)} %reshape.172), calls=%async_computation.3 | async-start | bytes 524288 | tf_op jit(solution)/shard_map/all_to_all | solution.py:109
  71.4 2.3 reduce.4
  74.5 11.4 %all-to-all-done.3 = bf16[16,2,4096]{2,1,0:T(2,128)(2,1)S(1)} async-done(((bf16[16,2,4096]{2,1,0:T(2,128)(2,1)}), bf16[16,2,4096]{2,1,0:T(2,128)(2,1)S(1)}, u32[]{:S(2)}, u32[]{:S(2)}) %all-to-all-start.3) | async-done | bytes 262176 | tf_op jit(solution)/shard_map/all_to_all | solution.py:109
  85.8 5.1 %all-to-all-start = ((bf16[16,2,4096]{2,1,0:T(2,128)(2,1)}), bf16[16,2,4096]{2,1,0:T(2,128)(2,1)S(1)}, u32[]{:S(2)}, u32[]{:S(2)}) async-start(bf16[16,2,4096]{2,1,0:T(2,128)(2,1)} %reshape.168), calls=%async_computation | async-start | bytes 524288 | tf_op jit(solution)/shard_map/all_to_all | solution.py:107
  91.3 2.3 reduce.5
  94.4 11.2 %all-to-all-done = bf16[16,2,4096]{2,1,0:T(2,128)(2,1)S(1)} async-done(((bf16[16,2,4096]{2,1,0:T(2,128)(2,1)}), bf16[16,2,4096]{2,1,0:T(2,128)(2,1)S(1)}, u32[]{:S(2)}, u32[]{:S(2)}) %all-to-all-start) | async-done | bytes 262176 | tf_op jit(solution)/shard_map/all_to_all | solution.py:107
  105.7 5.2 %all-to-all-start.1 = ((bf16[16,2,4096]{2,1,0:T(2,128)(2,1)}), bf16[16,2,4096]{2,1,0:T(2,128)(2,1)S(1)}, u32[]{:S(2)}, u32[]{:S(2)}) async-start(bf16[16,2,4096]{2,1,0:T(2,128)(2,1)} %reshape.170), calls=%async_computation.1 | async-start | bytes 524288 | tf_op jit(solution)/shard_map/all_to_all | solution.py:108
  114.0 11.4 %all-to-all-done.1 = bf16[16,2,4096]{2,1,0:T(2,128)(2,1)S(1)} async-done(((bf16[16,2,4096]{2,1,0:T(2,128)(2,1)}), bf16[16,2,4096]{2,1,0:T(2,128)(2,1)S(1)}, u32[]{:S(2)}, u32[]{:S(2)}) %all-to-all-start.1) | async-done | bytes 262176 | tf_op jit(solution)/shard_map/all_to_all | solution.py:108
  126.8 117.7 %while.24 = (s32[]{:T(128)}, f32[4,1,512,64]{2,3,1,0:T(8,128)}, s32[4]{0:T(128)S(1)}, bf16[1,4,512,64]{3,2,1,0:T(8,128)(2,1)}, bf16[1,2048,64]{2,1,0:T(8,128)(2,...) while((s32[]{:T(128)}, f32[4,1,512,64]{2,3,1,0:T(8,128)}, ...), condition=%wide.region_6.7_spmd, body=%wide.region_0.6_spmd.sunk | while | flops 109617680 | bytes 10642510 | solution.py:64
  131.5 9.6 %while.25 = (s32[]{:T(128)}, f32[1,512,64]{1,2,0:T(8,128)S(1)}, f32[1,512,1]{1,2,0:T(1,128)S(1)}, s32[]{:T(128)}, s32[]{:T(128)}, /*index=5*/bf16[1,2048,64]{2,1...) while((s32[]{:T(128)}, f32[1,512,64]{1,2,0:T(8,128)S(1)}, ...), condition=%wide.region_5.5_spmd.clone, body=%wide.region_1.4_spmd.clone.sunk | while | flops 109617672 | bytes 10115295 | solution.py:61
  132.1 1.9 fusion.42
  134.0 4.8 %fusion.43 = f32[1,512,4,128]{1,2,3,0:T(4,128)S(1)} fusion(f32[1,512,4,128]{1,3,2,0:T(8,128)S(1)} %bitcast.136), kind=kOutput, calls=%fused_computation.18.clone.1 | output fusion | flops 33292288 | bytes 2097152 | tf_op jit(solution)/shard_map/reduce-window
  139.2 1.6 fusion.44
  146.5 19.2 %while.25 = (s32[]{:T(128)}, f32[1,512,64]{1,2,0:T(8,128)S(1)}, f32[1,512,1]{1,2,0:T(1,128)S(1)}, s32[]{:T(128)}, s32[]{:T(128)}, /*index=5*/bf16[1,2048,64]{2,1...) while((s32[]{:T(128)}, f32[1,512,64]{1,2,0:T(8,128)S(1)}, ...), condition=%wide.region_5.5_spmd.clone, body=%wide.region_1.4_spmd.clone.sunk | while | flops 109617672 | bytes 10115295 | solution.py:61
  147.1 1.9 fusion.42
  149.0 4.8 %fusion.43 = f32[1,512,4,128]{1,2,3,0:T(4,128)S(1)} fusion(f32[1,512,4,128]{1,3,2,0:T(8,128)S(1)} %bitcast.136), kind=kOutput, calls=%fused_computation.18.clone.1 | output fusion | flops 33292288 | bytes 2097152 | tf_op jit(solution)/shard_map/reduce-window
  154.2 1.6 fusion.44
  156.7 1.9 fusion.42
  158.6 4.8 %fusion.43 = f32[1,512,4,128]{1,2,3,0:T(4,128)S(1)} fusion(f32[1,512,4,128]{1,3,2,0:T(8,128)S(1)} %bitcast.136), kind=kOutput, calls=%fused_computation.18.clone.1 | output fusion | flops 33292288 | bytes 2097152 | tf_op jit(solution)/shard_map/reduce-window
  163.8 1.6 fusion.44
  171.1 28.9 %while.25 = (s32[]{:T(128)}, f32[1,512,64]{1,2,0:T(8,128)S(1)}, f32[1,512,1]{1,2,0:T(1,128)S(1)}, s32[]{:T(128)}, s32[]{:T(128)}, /*index=5*/bf16[1,2048,64]{2,1...) while((s32[]{:T(128)}, f32[1,512,64]{1,2,0:T(8,128)S(1)}, ...), condition=%wide.region_5.5_spmd.clone, body=%wide.region_1.4_spmd.clone.sunk | while | flops 109617672 | bytes 10115295 | solution.py:61
  171.7 1.9 fusion.42
  173.6 4.8 %fusion.43 = f32[1,512,4,128]{1,2,3,0:T(4,128)S(1)} fusion(f32[1,512,4,128]{1,3,2,0:T(8,128)S(1)} %bitcast.136), kind=kOutput, calls=%fused_computation.18.clone.1 | output fusion | flops 33292288 | bytes 2097152 | tf_op jit(solution)/shard_map/reduce-window
  178.8 1.6 fusion.44
  181.4 1.9 fusion.42
  183.2 4.8 %fusion.43 = f32[1,512,4,128]{1,2,3,0:T(4,128)S(1)} fusion(f32[1,512,4,128]{1,3,2,0:T(8,128)S(1)} %bitcast.136), kind=kOutput, calls=%fused_computation.18.clone.1 | output fusion | flops 33292288 | bytes 2097152 | tf_op jit(solution)/shard_map/reduce-window
  188.4 1.6 fusion.44
  191.0 1.9 fusion.42
  192.8 4.8 %fusion.43 = f32[1,512,4,128]{1,2,3,0:T(4,128)S(1)} fusion(f32[1,512,4,128]{1,3,2,0:T(8,128)S(1)} %bitcast.136), kind=kOutput, calls=%fused_computation.18.clone.1 | output fusion | flops 33292288 | bytes 2097152 | tf_op jit(solution)/shard_map/reduce-window
  198.1 1.6 fusion.44
  205.3 38.5 %while.25 = (s32[]{:T(128)}, f32[1,512,64]{1,2,0:T(8,128)S(1)}, f32[1,512,1]{1,2,0:T(1,128)S(1)}, s32[]{:T(128)}, s32[]{:T(128)}, /*index=5*/bf16[1,2048,64]{2,1...) while((s32[]{:T(128)}, f32[1,512,64]{1,2,0:T(8,128)S(1)}, ...), condition=%wide.region_5.5_spmd.clone, body=%wide.region_1.4_spmd.clone.sunk | while | flops 109617672 | bytes 10115295 | solution.py:61
  206.0 1.9 fusion.42
  207.8 4.8 %fusion.43 = f32[1,512,4,128]{1,2,3,0:T(4,128)S(1)} fusion(f32[1,512,4,128]{1,3,2,0:T(8,128)S(1)} %bitcast.136), kind=kOutput, calls=%fused_computation.18.clone.1 | output fusion | flops 33292288 | bytes 2097152 | tf_op jit(solution)/shard_map/reduce-window
  213.0 1.6 fusion.44
  215.6 1.9 fusion.42
  217.5 4.8 %fusion.43 = f32[1,512,4,128]{1,2,3,0:T(4,128)S(1)} fusion(f32[1,512,4,128]{1,3,2,0:T(8,128)S(1)} %bitcast.136), kind=kOutput, calls=%fused_computation.18.clone.1 | output fusion | flops 33292288 | bytes 2097152 | tf_op jit(solution)/shard_map/reduce-window
  225.2 1.9 fusion.42
  227.1 4.8 %fusion.43 = f32[1,512,4,128]{1,2,3,0:T(4,128)S(1)} fusion(f32[1,512,4,128]{1,3,2,0:T(8,128)S(1)} %bitcast.136), kind=kOutput, calls=%fused_computation.18.clone.1 | output fusion | flops 33292288 | bytes 2097152 | tf_op jit(solution)/shard_map/reduce-window
  234.8 1.9 fusion.42
  236.7 4.8 %fusion.43 = f32[1,512,4,128]{1,2,3,0:T(4,128)S(1)} fusion(f32[1,512,4,128]{1,3,2,0:T(8,128)S(1)} %bitcast.136), kind=kOutput, calls=%fused_computation.18.clone.1 | output fusion | flops 33292288 | bytes 2097152 | tf_op jit(solution)/shard_map/reduce-window
  247.4 11.8 %reduce.7 = bf16[2048,64]{1,0:T(8,128)(2,1)S(1)} reduce(bf16[2048,1,64]{2,1,0:T(2,128)(2,1)S(1)} %bitcast.140, bf16[]{:T(256)} %broadcast.71), dimensions={1}, to_apply=%bitcast.94.reduce_sub_computation | reduce | bytes 524290
  259.6 20.0 %all_to_all.69 = bf16[16,2,4096]{2,1,0:T(2,128)(2,1)S(1)} all-to-all(bf16[16,2,4096]{2,1,0:T(2,128)(2,1)S(1)} %reshape.174), channel_id=1, replica_groups=mesh['sp'=16,'dp'=32] {'sp'}, dimensions={0} | all-to-all | bytes 524288 | tf_op jit(solution)/shard_map/all_to_all | solution.py:113
  281.2 3.5 %fusion.24 = bf16[128,1024]{0,1:T(8,128)(2,1)S(1)} fusion(f32[1,128,16,64]{1,3,2,0:T(8,128)S(1)} %copy.87, bf16[2048,1024]{1,0:T(8,128)(2,1)} %all-gather.3.cloned.1.call-done, bf16[1,128,2048]{2,1,0:T(8,128)(2,1)S(1)} %copy-done), kind=kOutput, calls=%fused_computation.40 | convolution fusion | flops 537657344 | bytes 5505024 | tf_op jit(solution)/shard_map/dot_general | solution.py:99
  284.7 4.5 %fusion.22 = bf16[1,128,2048]{2,1,0:T(8,128)(2,1)} fusion(bf16[128,1024]{0,1:T(8,128)(2,1)S(1)} %fusion.24, bf16[1024,2048]{0,1:T(8,128)(2,1)} %all-gather.5.cloned.1.call-done), kind=kOutput, calls=%fused_computation.36 | convolution fusion | flops 537133056 | bytes 4980736 | tf_op jit(solution)/shard_map/dot_general | solution.py:115
  (152 shorter events, 38.7 us)
Async XLA Ops:
  6.5 274.7 %copy-start = (bf16[1,128,2048]{2,1,0:T(8,128)(2,1)S(1)}, bf16[1,128,2048]{2,1,0:T(8,128)(2,1)}, u32[]{:S(2)}) copy-start(bf16[1,128,2048]{2,1,0:T(8,128)(2,1)} %param.15) | copy-start | bytes 1572868
  6.5 64.4 %copy-start.1 = (bf16[1,128,1024]{2,1,0:T(8,128)(2,1)S(1)}, bf16[1,128,1024]{2,1,0:T(8,128)(2,1)}, u32[]{:S(2)}) copy-start(bf16[1,128,1024]{2,1,0:T(8,128)(2,1)} %param.11) | copy-start | bytes 786436
  6.5 84.4 %copy-start.2 = (bf16[1,128,1024]{2,1,0:T(8,128)(2,1)S(1)}, bf16[1,128,1024]{2,1,0:T(8,128)(2,1)}, u32[]{:S(2)}) copy-start(bf16[1,128,1024]{2,1,0:T(8,128)(2,1)} %param.12) | copy-start | bytes 786436
  6.5 274.6 %all-gather.3.cloned.1.call-start = ((), (), s32[]{:S(2)}) async-start(), calls=%async_computation.5 | async-start | bytes 4325376 | tf_op jit(solution)/shard_map/all_gather | solution.py:101
  45.1 19.9 %all-to-all-start.2 = ((bf16[1,128,16]{1,0,2:T(2,128)(2,1)}), bf16[1,128,16]{1,0,2:T(2,128)(2,1)S(1)}, u32[]{:S(2)}, u32[]{:S(2)}) async-start(bf16[1,128,16]{1,0,2:T(2,128)(2,1)} %copy.78), calls=%async_computation.2 | async-start | bytes 16384 | tf_op jit(solution)/shard_map/all_to_all | solution.py:110
  65.1 20.8 %all-to-all-start.3 = ((bf16[16,2,4096]{2,1,0:T(2,128)(2,1)}), bf16[16,2,4096]{2,1,0:T(2,128)(2,1)S(1)}, u32[]{:S(2)}, u32[]{:S(2)}) async-start(bf16[16,2,4096]{2,1,0:T(2,128)(2,1)} %reshape.172), calls=%async_computation.3 | async-start | bytes 524288 | tf_op jit(solution)/shard_map/all_to_all | solution.py:109
  85.8 19.8 %all-to-all-start = ((bf16[16,2,4096]{2,1,0:T(2,128)(2,1)}), bf16[16,2,4096]{2,1,0:T(2,128)(2,1)S(1)}, u32[]{:S(2)}, u32[]{:S(2)}) async-start(bf16[16,2,4096]{2,1,0:T(2,128)(2,1)} %reshape.168), calls=%async_computation | async-start | bytes 524288 | tf_op jit(solution)/shard_map/all_to_all | solution.py:107
  105.7 19.7 %all-to-all-start.1 = ((bf16[16,2,4096]{2,1,0:T(2,128)(2,1)}), bf16[16,2,4096]{2,1,0:T(2,128)(2,1)S(1)}, u32[]{:S(2)}, u32[]{:S(2)}) async-start(bf16[16,2,4096]{2,1,0:T(2,128)(2,1)} %reshape.170), calls=%async_computation.1 | async-start | bytes 524288 | tf_op jit(solution)/shard_map/all_to_all | solution.py:108
  110.9 173.8 %all-gather.5.cloned.1.call-start = ((), (), s32[]{:S(2)}) async-start(), calls=%async_computation.6 | async-start | bytes 4325376 | tf_op jit(solution)/shard_map/all_gather | solution.py:117
Sparse Core Ops, SparseCore 0:
  44.0 56.9 all-gather.2
  114.8 60.2 all-gather.4
where the time goes:
time: 297 us; the launch traced here: 296 us
  other arithmetic  84.9 us (29%)
  blocking collectives  54.6 us (18%)
  waiting for transfers between devices  40.2 us (14%)
  matrix products  29.4 us (10%)
  local copies, waits for them, and re-layouts  28.5 us (10%)
  starting transfers between devices  25.3 us (9%)
  loops' own time  19.6 us (7%)
  between operations  13.6 us (5%)
    another operation x20, other arithmetic  48.3 us
    all_gather x1, blocking collectives, turned_gather(): out = lax.all_gather(both, axis, axis=0, tiled=True)  34.7 us
    all_to_all x1, blocking collectives, shards(): lax.all_to_all(normed, 'sp', split_axis=1, concat_axis=2, tiled=True)  20 us
    unnamed x6, other arithmetic  18.8 us
    dot_general x10, matrix products, key_step(): jnp.einsum('gqd,gkd->gqk', query_block, key_block, preferred_element_type...  18.7 us
    convert_element_type x10, other arithmetic, key_step(): weights = jnp.where(earlier, jnp.exp(jax.nn.log_sigmoid(scores) + later_s...  15.7 us
    another operation x1, loops' own time, stick_blocks(): outputs = lax.map(one_block, jnp.arange(block_count, dtype=jnp.int32))  12.5 us
    all_to_all x1, waiting for transfers between devices, shards(): lax.all_to_all(value_rows, 'sp', split_axis=2, concat_axis=1, tiled=True)  11.4 us
  transfers between devices with their start and end apart: 6, of which 4 were waited for; matrix products, arithmetic and copies ran while one was open for 46% of the time, Pallas kernels for 0%

commit v1 on v0

--- a/solution.py
+++ b/solution.py
@@ -10,7 +10,9 @@
     turned = [jnp.moveaxis(a, dim, 0) for a, dim in zip(arrays, dims)]
     widths = [t[0].size for t in turned]
     both = jnp.concatenate([t.reshape(-1, w) for t, w in zip(turned, widths)], axis=1)
-    out = lax.all_gather(both, axis, axis=0, tiled=True)
+    out = jnp.concatenate(
+        lax.all_to_all(jnp.stack([both] * lax.axis_size(axis)), axis, 0, 0), axis=0
+    )
     blocks = jnp.split(out, [sum(widths[:k]) for k in range(1, len(widths))], axis=1)
     return tuple(
         (

time: 297 us -> 309 us (1.040)
  the two profiles are of different devices: /device:TPU:54 before, /device:TPU:10 now
where the time goes in v1:
time: 309 us; the launch traced here: 308 us
  other arithmetic  84.9 us (27%)
  blocking collectives  57.3 us (19%)
  waiting for transfers between devices  53.2 us (17%)
  matrix products  29.4 us (10%)
  local copies, waits for them, and re-layouts  28.5 us (9%)
  starting transfers between devices  21.4 us (7%)
  loops' own time  19.6 us (6%)
  between operations  13.7 us (4%)
    another operation x20, other arithmetic  48.3 us
    all_to_all x1, blocking collectives, turned_gather(): lax.all_to_all(jnp.stack([both] * lax.axis_size(axis)), axis, 0, 0)  33.4 us
    all_to_all x1, blocking collectives, shards(): lax.all_to_all(normed, 'sp', split_axis=1, concat_axis=2, tiled=True)  23.9 us
    unnamed x6, other arithmetic  18.8 us
    dot_general x10, matrix products, key_step(): jnp.einsum('gqd,gkd->gqk', query_block, key_block, preferred_element_type...  18.7 us
    all_to_all x1, waiting for transfers between devices, shards(): lax.all_to_all(key_rows, 'sp', split_axis=2, concat_axis=1, tiled=True)  16.2 us
    convert_element_type x10, other arithmetic, key_step(): weights = jnp.where(earlier, jnp.exp(jax.nn.log_sigmoid(scores) + later_s...  15.7 us
    all_to_all x1, waiting for transfers between devices, shards(): lax.all_to_all(queries, 'sp', split_axis=2, concat_axis=1, tiled=True)  14.8 us
  transfers between devices with their start and end apart: 6, of which 4 were waited for; matrix products, arithmetic and copies ran while one was open for 44% of the time, Pallas kernels for 0%

profile of v1, /device:TPU:10, one launch (start us, length us, event | category | flops | bytes accessed | tf_op | source)
XLA Modules:
  0.0 308.0 jit_solution(10103287003376177400)
XLA Ops:
  8.3 33.4 %all_to_all.74 = bf16[16,64,128]{2,1,0:T(8,128)(2,1)S(1)} all-to-all(bf16[16,64,128]{2,1,0:T(8,128)(2,1)S(1)} %stack.2), channel_id=1, replica_groups=mesh['sp'=16,'dp'=32] {'sp'}, dimensions={0} | all-to-all | bytes 524288 | tf_op jit(solution)/shard_map/all_to_all | solution.py:14
  43.9 5.8 %all-to-all-start.2 = ((bf16[1,128,16]{1,0,2:T(2,128)(2,1)}), bf16[1,128,16]{1,0,2:T(2,128)(2,1)S(1)}, u32[]{:S(2)}, u32[]{:S(2)}) async-start(bf16[1,128,16]{1,0,2:T(2,128)(2,1)} %copy.79), calls=%async_computation.2 | async-start | bytes 16384 | tf_op jit(solution)/shard_map/all_to_all | solution.py:112
  51.6 2.3 reduce.6
  54.6 7.5 %all-to-all-done.2 = bf16[1,128,16]{1,0,2:T(2,128)(2,1)S(1)} async-done(((bf16[1,128,16]{1,0,2:T(2,128)(2,1)}), bf16[1,128,16]{1,0,2:T(2,128)(2,1)S(1)}, u32[]{:S(2)}, u32[]{:S(2)}) %all-to-all-start.2) | async-done | bytes 4128 | tf_op jit(solution)/shard_map/all_to_all | solution.py:112
  62.1 4.6 %all-to-all-start.3 = ((bf16[16,2,4096]{2,1,0:T(2,128)(2,1)}), bf16[16,2,4096]{2,1,0:T(2,128)(2,1)S(1)}, u32[]{:S(2)}, u32[]{:S(2)}) async-start(bf16[16,2,4096]{2,1,0:T(2,128)(2,1)} %reshape.178), calls=%async_computation.3 | async-start | bytes 524288 | tf_op jit(solution)/shard_map/all_to_all | solution.py:111
  67.1 2.3 reduce.4
  70.2 14.7 %all-to-all-done.3 = bf16[16,2,4096]{2,1,0:T(2,128)(2,1)S(1)} async-done(((bf16[16,2,4096]{2,1,0:T(2,128)(2,1)}), bf16[16,2,4096]{2,1,0:T(2,128)(2,1)S(1)}, u32[]{:S(2)}, u32[]{:S(2)}) %all-to-all-start.3) | async-done | bytes 262176 | tf_op jit(solution)/shard_map/all_to_all | solution.py:111
  84.8 5.4 %all-to-all-start = ((bf16[16,2,4096]{2,1,0:T(2,128)(2,1)}), bf16[16,2,4096]{2,1,0:T(2,128)(2,1)S(1)}, u32[]{:S(2)}, u32[]{:S(2)}) async-start(bf16[16,2,4096]{2,1,0:T(2,128)(2,1)} %reshape.174), calls=%async_computation | async-start | bytes 524288 | tf_op jit(solution)/shard_map/all_to_all | solution.py:109
  90.6 2.3 reduce.5
  93.7 14.8 %all-to-all-done = bf16[16,2,4096]{2,1,0:T(2,128)(2,1)S(1)} async-done(((bf16[16,2,4096]{2,1,0:T(2,128)(2,1)}), bf16[16,2,4096]{2,1,0:T(2,128)(2,1)S(1)}, u32[]{:S(2)}, u32[]{:S(2)}) %all-to-all-start) | async-done | bytes 262176 | tf_op jit(solution)/shard_map/all_to_all | solution.py:109
  108.4 5.5 %all-to-all-start.1 = ((bf16[16,2,4096]{2,1,0:T(2,128)(2,1)}), bf16[16,2,4096]{2,1,0:T(2,128)(2,1)S(1)}, u32[]{:S(2)}, u32[]{:S(2)}) async-start(bf16[16,2,4096]{2,1,0:T(2,128)(2,1)} %reshape.176), calls=%async_computation.1 | async-start | bytes 524288 | tf_op jit(solution)/shard_map/all_to_all | solution.py:110
  116.2 16.2 %all-to-all-done.1 = bf16[16,2,4096]{2,1,0:T(2,128)(2,1)S(1)} async-done(((bf16[16,2,4096]{2,1,0:T(2,128)(2,1)}), bf16[16,2,4096]{2,1,0:T(2,128)(2,1)S(1)}, u32[]{:S(2)}, u32[]{:S(2)}) %all-to-all-start.1) | async-done | bytes 262176 | tf_op jit(solution)/shard_map/all_to_all | solution.py:110
  134.7 117.7 %while.24 = (s32[]{:T(128)}, f32[4,1,512,64]{2,3,1,0:T(8,128)}, s32[4]{0:T(128)S(1)}, bf16[1,4,512,64]{3,2,1,0:T(8,128)(2,1)}, bf16[1,2048,64]{2,1,0:T(8,128)(2,...) while((s32[]{:T(128)}, f32[4,1,512,64]{2,3,1,0:T(8,128)}, ...), condition=%wide.region_6.7_spmd, body=%wide.region_0.6_spmd.sunk | while | flops 109617680 | bytes 10642510 | solution.py:66
  139.4 9.6 %while.25 = (s32[]{:T(128)}, f32[1,512,64]{1,2,0:T(8,128)S(1)}, f32[1,512,1]{1,2,0:T(1,128)S(1)}, s32[]{:T(128)}, s32[]{:T(128)}, /*index=5*/bf16[1,2048,64]{2,1...) while((s32[]{:T(128)}, f32[1,512,64]{1,2,0:T(8,128)S(1)}, ...), condition=%wide.region_5.5_spmd.clone, body=%wide.region_1.4_spmd.clone.sunk | while | flops 109617672 | bytes 10115295 | solution.py:63
  140.1 1.9 fusion.42
  142.0 4.8 %fusion.43 = f32[1,512,4,128]{1,2,3,0:T(4,128)S(1)} fusion(f32[1,512,4,128]{1,3,2,0:T(8,128)S(1)} %bitcast.137), kind=kOutput, calls=%fused_computation.18.clone.1 | output fusion | flops 33292288 | bytes 2097152 | tf_op jit(solution)/shard_map/reduce-window
  147.2 1.6 fusion.44
  154.4 19.2 %while.25 = (s32[]{:T(128)}, f32[1,512,64]{1,2,0:T(8,128)S(1)}, f32[1,512,1]{1,2,0:T(1,128)S(1)}, s32[]{:T(128)}, s32[]{:T(128)}, /*index=5*/bf16[1,2048,64]{2,1...) while((s32[]{:T(128)}, f32[1,512,64]{1,2,0:T(8,128)S(1)}, ...), condition=%wide.region_5.5_spmd.clone, body=%wide.region_1.4_spmd.clone.sunk | while | flops 109617672 | bytes 10115295 | solution.py:63
  155.1 1.9 fusion.42
  156.9 4.8 %fusion.43 = f32[1,512,4,128]{1,2,3,0:T(4,128)S(1)} fusion(f32[1,512,4,128]{1,3,2,0:T(8,128)S(1)} %bitcast.137), kind=kOutput, calls=%fused_computation.18.clone.1 | output fusion | flops 33292288 | bytes 2097152 | tf_op jit(solution)/shard_map/reduce-window
  162.1 1.6 fusion.44
  164.7 1.9 fusion.42
  166.6 4.8 %fusion.43 = f32[1,512,4,128]{1,2,3,0:T(4,128)S(1)} fusion(f32[1,512,4,128]{1,3,2,0:T(8,128)S(1)} %bitcast.137), kind=kOutput, calls=%fused_computation.18.clone.1 | output fusion | flops 33292288 | bytes 2097152 | tf_op jit(solution)/shard_map/reduce-window
  171.8 1.6 fusion.44
  179.0 28.9 %while.25 = (s32[]{:T(128)}, f32[1,512,64]{1,2,0:T(8,128)S(1)}, f32[1,512,1]{1,2,0:T(1,128)S(1)}, s32[]{:T(128)}, s32[]{:T(128)}, /*index=5*/bf16[1,2048,64]{2,1...) while((s32[]{:T(128)}, f32[1,512,64]{1,2,0:T(8,128)S(1)}, ...), condition=%wide.region_5.5_spmd.clone, body=%wide.region_1.4_spmd.clone.sunk | while | flops 109617672 | bytes 10115295 | solution.py:63
  179.7 1.9 fusion.42
  181.6 4.8 %fusion.43 = f32[1,512,4,128]{1,2,3,0:T(4,128)S(1)} fusion(f32[1,512,4,128]{1,3,2,0:T(8,128)S(1)} %bitcast.137), kind=kOutput, calls=%fused_computation.18.clone.1 | output fusion | flops 33292288 | bytes 2097152 | tf_op jit(solution)/shard_map/reduce-window
  186.8 1.6 fusion.44
  189.3 1.9 fusion.42
  191.2 4.8 %fusion.43 = f32[1,512,4,128]{1,2,3,0:T(4,128)S(1)} fusion(f32[1,512,4,128]{1,3,2,0:T(8,128)S(1)} %bitcast.137), kind=kOutput, calls=%fused_computation.18.clone.1 | output fusion | flops 33292288 | bytes 2097152 | tf_op jit(solution)/shard_map/reduce-window
  196.4 1.6 fusion.44
  198.9 1.9 fusion.42
  200.8 4.8 %fusion.43 = f32[1,512,4,128]{1,2,3,0:T(4,128)S(1)} fusion(f32[1,512,4,128]{1,3,2,0:T(8,128)S(1)} %bitcast.137), kind=kOutput, calls=%fused_computation.18.clone.1 | output fusion | flops 33292288 | bytes 2097152 | tf_op jit(solution)/shard_map/reduce-window
  206.0 1.6 fusion.44
  213.2 38.5 %while.25 = (s32[]{:T(128)}, f32[1,512,64]{1,2,0:T(8,128)S(1)}, f32[1,512,1]{1,2,0:T(1,128)S(1)}, s32[]{:T(128)}, s32[]{:T(128)}, /*index=5*/bf16[1,2048,64]{2,1...) while((s32[]{:T(128)}, f32[1,512,64]{1,2,0:T(8,128)S(1)}, ...), condition=%wide.region_5.5_spmd.clone, body=%wide.region_1.4_spmd.clone.sunk | while | flops 109617672 | bytes 10115295 | solution.py:63
  213.9 1.9 fusion.42
  215.8 4.8 %fusion.43 = f32[1,512,4,128]{1,2,3,0:T(4,128)S(1)} fusion(f32[1,512,4,128]{1,3,2,0:T(8,128)S(1)} %bitcast.137), kind=kOutput, calls=%fused_computation.18.clone.1 | output fusion | flops 33292288 | bytes 2097152 | tf_op jit(solution)/shard_map/reduce-window
  221.0 1.6 fusion.44
  223.5 1.9 fusion.42
  225.4 4.8 %fusion.43 = f32[1,512,4,128]{1,2,3,0:T(4,128)S(1)} fusion(f32[1,512,4,128]{1,3,2,0:T(8,128)S(1)} %bitcast.137), kind=kOutput, calls=%fused_computation.18.clone.1 | output fusion | flops 33292288 | bytes 2097152 | tf_op jit(solution)/shard_map/reduce-window
  233.1 1.9 fusion.42
  235.0 4.8 %fusion.43 = f32[1,512,4,128]{1,2,3,0:T(4,128)S(1)} fusion(f32[1,512,4,128]{1,3,2,0:T(8,128)S(1)} %bitcast.137), kind=kOutput, calls=%fused_computation.18.clone.1 | output fusion | flops 33292288 | bytes 2097152 | tf_op jit(solution)/shard_map/reduce-window
  242.7 1.9 fusion.42
  244.6 4.8 %fusion.43 = f32[1,512,4,128]{1,2,3,0:T(4,128)S(1)} fusion(f32[1,512,4,128]{1,3,2,0:T(8,128)S(1)} %bitcast.137), kind=kOutput, calls=%fused_computation.18.clone.1 | output fusion | flops 33292288 | bytes 2097152 | tf_op jit(solution)/shard_map/reduce-window
  255.4 11.8 %reduce.7 = bf16[2048,64]{1,0:T(8,128)(2,1)S(1)} reduce(bf16[2048,1,64]{2,1,0:T(2,128)(2,1)S(1)} %bitcast.141, bf16[]{:T(256)} %broadcast.73), dimensions={1}, to_apply=%bitcast.95.reduce_sub_computation | reduce | bytes 524290
  267.6 23.9 %all_to_all.75 = bf16[16,2,4096]{2,1,0:T(2,128)(2,1)S(1)} all-to-all(bf16[16,2,4096]{2,1,0:T(2,128)(2,1)S(1)} %reshape.180), channel_id=1, replica_groups=mesh['sp'=16,'dp'=32] {'sp'}, dimensions={0} | all-to-all | bytes 524288 | tf_op jit(solution)/shard_map/all_to_all | solution.py:115
  293.1 3.5 %fusion.24 = bf16[128,1024]{0,1:T(8,128)(2,1)S(1)} fusion(f32[1,128,16,64]{1,3,2,0:T(8,128)S(1)} %copy.88, bf16[2048,1024]{1,0:T(8,128)(2,1)} %all-gather.3.cloned.1.call-done, bf16[1,128,2048]{2,1,0:T(8,128)(2,1)S(1)} %copy-done), kind=kOutput, calls=%fused_computation.40 | convolution fusion | flops 537657344 | bytes 5505024 | tf_op jit(solution)/shard_map/dot_general | solution.py:101
  296.6 4.5 %fusion.22 = bf16[1,128,2048]{2,1,0:T(8,128)(2,1)} fusion(bf16[128,1024]{0,1:T(8,128)(2,1)S(1)} %fusion.24, bf16[1024,2048]{0,1:T(8,128)(2,1)} %all-gather.5.cloned.1.call-done), kind=kOutput, calls=%fused_computation.36 | convolution fusion | flops 537133056 | bytes 4980736 | tf_op jit(solution)/shard_map/dot_general | solution.py:117
  (153 shorter events, 38.7 us)
Async XLA Ops:
  6.5 286.5 %copy-start = (bf16[1,128,2048]{2,1,0:T(8,128)(2,1)S(1)}, bf16[1,128,2048]{2,1,0:T(8,128)(2,1)}, u32[]{:S(2)}) copy-start(bf16[1,128,2048]{2,1,0:T(8,128)(2,1)} %param.15) | copy-start | bytes 1572868
  6.5 60.1 %copy-start.1 = (bf16[1,128,1024]{2,1,0:T(8,128)(2,1)S(1)}, bf16[1,128,1024]{2,1,0:T(8,128)(2,1)}, u32[]{:S(2)}) copy-start(bf16[1,128,1024]{2,1,0:T(8,128)(2,1)} %param.11) | copy-start | bytes 786436
  6.5 83.7 %copy-start.2 = (bf16[1,128,1024]{2,1,0:T(8,128)(2,1)S(1)}, bf16[1,128,1024]{2,1,0:T(8,128)(2,1)}, u32[]{:S(2)}) copy-start(bf16[1,128,1024]{2,1,0:T(8,128)(2,1)} %param.12) | copy-start | bytes 786436
  6.5 286.5 %all-gather.3.cloned.1.call-start = ((), (), s32[]{:S(2)}) async-start(), calls=%async_computation.6 | async-start | bytes 4325376 | tf_op jit(solution)/shard_map/all_gather | solution.py:103
  43.9 18.2 %all-to-all-start.2 = ((bf16[1,128,16]{1,0,2:T(2,128)(2,1)}), bf16[1,128,16]{1,0,2:T(2,128)(2,1)S(1)}, u32[]{:S(2)}, u32[]{:S(2)}) async-start(bf16[1,128,16]{1,0,2:T(2,128)(2,1)} %copy.79), calls=%async_computation.2 | async-start | bytes 16384 | tf_op jit(solution)/shard_map/all_to_all | solution.py:112
  62.1 22.7 %all-to-all-start.3 = ((bf16[16,2,4096]{2,1,0:T(2,128)(2,1)}), bf16[16,2,4096]{2,1,0:T(2,128)(2,1)S(1)}, u32[]{:S(2)}, u32[]{:S(2)}) async-start(bf16[16,2,4096]{2,1,0:T(2,128)(2,1)} %reshape.178), calls=%async_computation.3 | async-start | bytes 524288 | tf_op jit(solution)/shard_map/all_to_all | solution.py:111
  84.8 23.6 %all-to-all-start = ((bf16[16,2,4096]{2,1,0:T(2,128)(2,1)}), bf16[16,2,4096]{2,1,0:T(2,128)(2,1)S(1)}, u32[]{:S(2)}, u32[]{:S(2)}) async-start(bf16[16,2,4096]{2,1,0:T(2,128)(2,1)} %reshape.174), calls=%async_computation | async-start | bytes 524288 | tf_op jit(solution)/shard_map/all_to_all | solution.py:109
  108.4 24.0 %all-to-all-start.1 = ((bf16[16,2,4096]{2,1,0:T(2,128)(2,1)}), bf16[16,2,4096]{2,1,0:T(2,128)(2,1)S(1)}, u32[]{:S(2)}, u32[]{:S(2)}) async-start(bf16[16,2,4096]{2,1,0:T(2,128)(2,1)} %reshape.176), calls=%async_computation.1 | async-start | bytes 524288 | tf_op jit(solution)/shard_map/all_to_all | solution.py:110
  113.9 182.7 %all-gather.5.cloned.1.call-start = ((), (), s32[]{:S(2)}) async-start(), calls=%async_computation.7 | async-start | bytes 4325376 | tf_op jit(solution)/shard_map/all_gather | solution.py:119
Sparse Core Ops, SparseCore 0:
  42.7 54.7 all-gather.2
  134.8 54.5 all-gather.4
